TPU v7x, 32 devices: a whole 2x2x4 slice. The times are simulated.
32 devices in a mesh: grp: 2 (over y), kv: 4 (over z), tp: 4 (over x, core).
Axes of the slice: x: 2, y: 2, z: 4, core: 2. Of those that a mesh axis runs over, the one named last changes fastest.
Arguments:
- tokens: bfloat16 [32, 4096], P('grp', 'kv'), parts along dimension 0, may hold values from -16 to 16
- positions: int32 [32], P(('grp', 'kv')), parts along dimension 0, may hold values from 512 to 8191
- state: float32 [32, 16, 128, 128], P(('grp', 'kv'), 'tp'), parts along dimension 0, may hold values from -3 to 3
- norm_gain: float32 [4096], P('kv'), may hold values from 0.1 to 1.9
- w_query: bfloat16 [4096, 2048], P('kv', 'tp'), may hold values from -0.09375 to 0.09375
- w_key: bfloat16 [4096, 2048], P('kv', 'tp'), may hold values from -0.09375 to 0.09375
- w_value: bfloat16 [4096, 2048], P('kv', 'tp'), may hold values from -0.09375 to 0.09375
- w_gate: bfloat16 [4096, 2048], P('kv', 'tp'), may hold values from -0.09375 to 0.09375
- w_out: bfloat16 [2048, 4096], P('tp', 'kv'), may hold values from -0.125 to 0.125
- mlp_gain: float32 [4096], P('kv'), may hold values from 0.1 to 1.9
- w_up: bfloat16 [4096, 16384], P('kv', 'tp'), may hold values from -0.09375 to 0.09375
- w_down: bfloat16 [16384, 4096], P('tp', 'kv'), may hold values from -0.046875 to 0.046875
Outputs:
- layer_out: bfloat16 [32, 4096], P('grp', 'kv'), parts along dimension 0
- new_state: float32 [32, 16, 128, 128], P(('grp', 'kv'), 'tp'), parts along dimension 0
There are 2 independent parts, one for each index of `grp`. A program takes and returns all parts, laid end to end along the dimension named above; an argument that names none is the same for every part. Nothing has to cross between parts.
All inputs are finite; a program needn't handle non-finite values.
Results may differ from a plain program's by a relative error of at most 0.007.
Values may be sent and summed in bfloat16 or wider, within the bound.
A program may use at most 64 MiB of HBM per device.

v0:
```python
import jax
import jax.numpy as jnp
from jax import lax
from jax.sharding import PartitionSpec as P

D = 4096
HEADS = 16


def turn(values, positions):
    half = values.shape[-1] // 2
    freq = 10000.0 ** (-(jnp.arange(half, dtype=jnp.float32) * 2.0) / values.shape[-1])
    angle = positions.astype(jnp.float32)[:, None, None] * freq[None, None, :]
    cosine = jnp.cos(angle)
    sine = jnp.sin(angle)
    first = values[..., :half]
    second = values[..., half:]
    return jnp.concatenate(
        [first * cosine - second * sine, first * sine + second * cosine], axis=-1
    )


def shards(
    tokens,
    positions,
    state,
    norm_gain,
    w_query,
    w_key,
    w_value,
    w_gate,
    w_out,
    mlp_gain,
    w_up,
    w_down,
):
    local_seqs, head_dev, head_size, _ = state.shape
    inputs = tokens.astype(jnp.float32)
    squares = jnp.sum(inputs * inputs, axis=1)
    normed = (inputs * norm_gain).astype(jnp.bfloat16)
    terms = jnp.stack(
        [
            jnp.dot(normed, weight, preferred_element_type=jnp.float32)
            for weight in (w_query, w_key, w_value, w_gate)
        ],
        axis=1,
    )
    summed, total_sq = (
        lax.psum_scatter(terms, "kv", scatter_dimension=0, tiled=True),
        lax.psum_scatter(squares, "kv", scatter_dimension=0, tiled=True),
    )
    scale1 = lax.rsqrt(total_sq / D + 1e-06)
    summed = (summed * scale1[:, None, None]).reshape(local_seqs, 4, head_dev, head_size)
    query = turn(summed[:, 0], positions)
    key_rows = turn(summed[:, 1], positions) * head_size ** (-0.5)
    value = summed[:, 2]
    gate = summed[:, 3]
    heads = (lax.axis_index("tp") * head_dev + jnp.arange(head_dev)).astype(jnp.float32)
    gamma = 1.0 - 2.0 ** (-5.0 - 5.0 * heads / (HEADS - 1))
    new_state = gamma[None, :, None, None] * state + key_rows[:, :, :, None] * value[:, :, None, :]
    read = jnp.einsum("bhd,bhde->bhe", query, new_state, precision=lax.Precision.HIGHEST)
    read = read * lax.rsqrt(jnp.mean(read * read, axis=-1, keepdims=True) + 1e-06)
    retained = (
        (read * jax.nn.silu(gate)).reshape(local_seqs, head_dev * head_size).astype(jnp.bfloat16)
    )
    head_terms = jnp.dot(
        lax.all_gather(retained, "kv", axis=0, tiled=True),
        w_out,
        preferred_element_type=jnp.float32,
    )
    mixed = (inputs + lax.psum(head_terms, "tp")).astype(jnp.bfloat16)
    middle = mixed.astype(jnp.float32)
    squares2 = jnp.sum(middle * middle, axis=1)
    normed2 = (middle * mlp_gain).astype(jnp.bfloat16)
    upward = jnp.dot(normed2, w_up, preferred_element_type=jnp.float32)
    up_full, total_sq2 = lax.psum((upward, squares2), "kv")
    scale2 = lax.rsqrt(total_sq2 / D + 1e-06)
    hidden = jnp.square(jax.nn.relu(up_full * scale2[:, None])).astype(jnp.bfloat16)
    down_terms = jnp.dot(hidden, w_down, preferred_element_type=jnp.float32)
    layer_out = (middle + lax.psum(down_terms, "tp")).astype(jnp.bfloat16)
    return (layer_out, new_state)


def solution(mesh):
    return jax.shard_map(
        shards,
        mesh=mesh,
        in_specs=(
            P("grp", "kv"),
            P(("grp", "kv")),
            P(("grp", "kv"), "tp", None, None),
            P("kv"),
            P("kv", "tp"),
            P("kv", "tp"),
            P("kv", "tp"),
            P("kv", "tp"),
            P("tp", "kv"),
            P("kv"),
            P("kv", "tp"),
            P("tp", "kv"),
        ),
        out_specs=(P("grp", "kv"), P(("grp", "kv"), "tp", None, None)),
        check_vma=False,
    )
```

profile of v0, /device:TPU:0, one launch (start us, length us, event | category | flops | bytes accessed | tf_op | source)
XLA Modules:
  0.0 187.9 jit_solution(12907306079230193447)
XLA Ops:
  7.2 0.0 copy-start
  7.2 0.0 copy-start.2
  7.2 0.0 copy-start.3
  7.2 0.0 all-reduce.13.cloned.1.call-start
  7.2 1.6 convolution_bitcast_fusion.3
  8.8 1.5 convolution_bitcast_fusion.2
  10.3 1.5 convolution_bitcast_fusion.1
  11.8 1.5 convolution_bitcast_fusion
  13.4 0.7 pad_maximum_fusion
  14.0 0.0 all-reduce.13.cloned.1.call-update
  14.1 0.0 all-reduce.7.cloned.1.call-start
  14.1 0.9 fusion.4
  15.0 0.7 convert_element_type.40
  15.7 0.1 multiply_cosine_fusion
  15.8 1.2 dynamic-slice
  17.7 13.5 %all-reduce.1 = f32[16]{0:T(128)S(1)} all-reduce(f32[16]{0:T(128)S(1)} %fusion.4), channel_id=3, replica_groups=mesh['grp'=2,'kv'=4,'tp'=4] {'kv'}, use_global_device_ids=true, to_apply=%region_2.0.clone | all-reduce | flops 16 | bytes 128
  31.2 0.1 fusion.19
  31.3 20.3 %all-reduce.13.cloned.1.call-done = f32[16,4,512]{2,0,1:T(8,128)} async-done(((f32[16,4,512]{2,0,1:T(8,128)}), f32[16,4,512]{2,0,1:T(8,128)}) %all-reduce.13.cloned.1.call-update) | async-done | bytes 131088
  51.6 0.9 dynamic-slice_multiply_fusion
  52.5 0.1 multiply_subtract_fusion
  52.6 0.1 pad_maximum_fusion.1
  52.7 1.6 multiply_add_fusion
  54.3 0.0 copy-start.1
  54.3 1.0 fusion.22
  55.3 0.1 multiply_reduce_fusion
  55.4 0.1 fusion.17
  55.5 13.2 %all-gather = bf16[4,4,512]{2,1,0:T(4,128)(2,1)S(1)} all-gather(bf16[1,4,512]{2,1,0:T(4,128)(2,1)S(1)} %reshape.108), channel_id=1, replica_groups=mesh['grp'=2,'kv'=4,'tp'=4] {'kv'}, dimensions={0}, use_global_device_ids=true | all-gather | bytes 20480 | tf_op jit(solution)/shard_map/all_gather | solution.py:67
  68.7 0.0 copy-done
  68.7 0.9 fusion.23
  69.6 0.0 all-reduce.7.cloned.1.call-update
  69.6 0.0 all-reduce.9.cloned.1.call-start
  69.6 31.3 %all-reduce.7.cloned.1.call-done = f32[16,1024]{1,0:T(8,128)} async-done(((f32[16,1024]{1,0:T(8,128)}), f32[16,1024]{1,0:T(8,128)}) %all-reduce.7.cloned.1.call-update) | async-done | bytes 65552 | tf_op jit(solution)/shard_map/psum | solution.py:71
  101.0 0.0 copy-done.2
  101.0 1.0 fusion.7
  101.9 0.0 copy-done.3
  101.9 5.3 %fusion.9 = f32[16,4096]{1,0:T(8,128)} fusion(bf16[1024,4096]{1,0:T(8,128)(2,1)} %param.22, bf16[16,1024]{1,0:T(8,128)(2,1)S(1)} %get-tuple-element.3, f32[1024]{0:T(1024)S(1)} %copy-done.3), kind=kOutput, calls=%fused_computation.22 | convolution fusion | flops 134266880 | bytes 8687616 | tf_op jit(solution)/shard_map/dot_general | solution.py:75
  107.2 0.0 copy-done.1
  107.2 0.0 all-reduce.9.cloned.1.call-update
  107.2 0.0 all-reduce.11.cloned.1.call-start
  107.3 11.8 %psum.30 = f32[16]{0:T(128)S(1)} all-reduce(f32[16]{0:T(128)S(1)} %get-tuple-element.2), channel_id=1, replica_groups=mesh['grp'=2,'kv'=4,'tp'=4] {'kv'}, use_global_device_ids=true, to_apply=%region_7.8 | all-reduce | flops 16 | bytes 128 | tf_op jit(solution)/shard_map/psum | solution.py:76
  119.1 23.9 %all-reduce.9.cloned.1.call-done = f32[16,4096]{1,0:T(8,128)} async-done(((f32[16,4096]{1,0:T(8,128)}), f32[16,4096]{1,0:T(8,128)}) %all-reduce.9.cloned.1.call-update) | async-done | bytes 262160 | tf_op jit(solution)/shard_map/psum | solution.py:76
  143.0 5.3 %fusion = f32[16,1024]{1,0:T(8,128)} fusion(bf16[4096,1024]{1,0:T(8,128)(2,1)} %param.23, f32[16,4096]{1,0:T(8,128)} %all-reduce.9.cloned.1.call-done, f32[16]{0:T(128)S(1)} %add_rsqrt_fusion.1), kind=kOutput, calls=%fused_computation.6 | convolution fusion | flops 134479872 | bytes 8716352 | tf_op jit(solution)/shard_map/dot_general | solution.py:79
  148.3 0.0 all-reduce.11.cloned.1.call-update
  148.4 31.6 %all-reduce.11.cloned.1.call-done = f32[16,1024]{1,0:T(8,128)} async-done(((f32[16,1024]{1,0:T(8,128)}), f32[16,1024]{1,0:T(8,128)}) %all-reduce.11.cloned.1.call-update) | async-done | bytes 65552 | tf_op jit(solution)/shard_map/psum | solution.py:80
  179.9 1.5 fusion.8
  (8 shorter events, 0.1 us)
Async XLA Ops:
  7.2 61.5 %copy-start = (bf16[512,1024]{1,0:T(8,128)(2,1)S(1)}, bf16[512,1024]{1,0:T(8,128)(2,1)}, u32[]{:S(2)}) copy-start(bf16[512,1024]{1,0:T(8,128)(2,1)} %param.20) | copy-start | bytes 3145732
  7.2 93.8 %copy-start.2 = (bf16[16,1024]{1,0:T(8,128)(2,1)S(1)}, bf16[16,1024]{1,0:T(8,128)(2,1)}, u32[]{:S(2)}) copy-start(bf16[16,1024]{1,0:T(8,128)(2,1)} %param.12) | copy-start | bytes 98308
  7.2 94.7 %copy-start.3 = (f32[1024]{0:T(1024)S(1)}, f32[1024]{0:T(1024)}, u32[]{:S(2)}) copy-start(f32[1024]{0:T(1024)} %param.21) | copy-start | bytes 12292
  7.2 44.4 %all-reduce.13.cloned.1.call-start = ((), (), s32[]{:S(2)}) async-start(), calls=%async_computation.3 | async-start | bytes 262144
  14.1 86.9 %all-reduce.7.cloned.1.call-start = ((), (), s32[]{:S(2)}) async-start(), calls=%async_computation | async-start | bytes 131072 | tf_op jit(solution)/shard_map/psum | solution.py:71
  54.3 52.9 %copy-start.1 = (f32[4,4,128,128]{3,2,1,0:T(8,128)}, f32[4,4,128,128]{3,2,1,0:T(8,128)S(1)}, u32[]{:S(2)}) copy-start(f32[4,4,128,128]{3,2,1,0:T(8,128)S(1)} %multiply_add_fusion) | copy-start | bytes 3145732
  69.6 73.4 %all-reduce.9.cloned.1.call-start = ((), (), s32[]{:S(2)}) async-start(), calls=%async_computation.1 | async-start | bytes 524288 | tf_op jit(solution)/shard_map/psum | solution.py:76
  107.2 72.7 %all-reduce.11.cloned.1.call-start = ((), (), s32[]{:S(2)}) async-start(), calls=%async_computation.2 | async-start | bytes 131072 | tf_op jit(solution)/shard_map/psum | solution.py:80
Sparse Core Ops, SparseCore 0:
  14.2 37.3 all-reduce.12
  69.7 31.1 all-reduce.6
  107.4 35.5 all-reduce.8
  148.5 31.3 all-reduce.10
where the time goes:
time: 189 us; the launch traced here: 188 us
  waiting for transfers between devices  107 us (57%)
  blocking collectives  38.5 us (20%)
  matrix products  18.6 us (10%)
  between operations  14.5 us (8%)
  other arithmetic  7.69 us (4%)
    psum x1, waiting for transfers between devices, shards(): layer_out = (middle + lax.psum(down_terms, 'tp')).astype(jnp.bfloat16)  31.6 us
    psum x1, waiting for transfers between devices, shards(): mixed = (inputs + lax.psum(head_terms, 'tp')).astype(jnp.bfloat16)  31.3 us
    psum x1, waiting for transfers between devices, shards(): up_full, total_sq2 = lax.psum((upward, squares2), 'kv')  23.9 us
    unnamed x5, waiting for transfers between devices  20.4 us
    unnamed x1, blocking collectives  13.5 us
    all_gather x1, blocking collectives, shards(): lax.all_gather(retained, 'kv', axis=0, tiled=True)  13.2 us
    psum x1, blocking collectives, shards(): up_full, total_sq2 = lax.psum((upward, squares2), 'kv')  11.8 us
    dot_general x4, matrix products, shards(): jnp.dot(normed, weight, preferred_element_type=jnp.float32)  6.11 us
  transfers between devices with their start and end apart: 4, of which 4 were waited for; matrix products, arithmetic and copies ran while one was open for 2% of the time, Pallas kernels for 0%

commit v1 on v0

--- a/solution.py
+++ b/solution.py
@@ -77,7 +77,7 @@
     scale2 = lax.rsqrt(total_sq2 / D + 1e-06)
     hidden = jnp.square(jax.nn.relu(up_full * scale2[:, None])).astype(jnp.bfloat16)
     down_terms = jnp.dot(hidden, w_down, preferred_element_type=jnp.float32)
-    layer_out = (middle + lax.psum(down_terms, "tp")).astype(jnp.bfloat16)
+    layer_out = (middle + jnp.sum(lax.all_gather(down_terms, "tp"), axis=0)).astype(jnp.bfloat16)
     return (layer_out, new_state)
 
 

time: 189 us -> 161 us (0.85)
  waiting for transfers between devices: 107 us -> 75.6 us
  blocking collectives: 38.5 us -> 44.3 us
    psum x1 -> x0, waiting for transfers between devices: 31.6 us -> none  [shards(): layer_out = (middle + lax.psum(down_terms, 'tp')).astype(jnp.bfloat16)]
    all_gather x0 -> x1, blocking collectives: none -> 5.77 us  [shards(): lax.all_gather(down_terms, 'tp')]
    unnamed x5 -> x4, waiting for transfers between devices: 20.4 us -> 20.4 us
  transfers between devices with their start and end apart: 4 -> 3, of which waited for: 4 -> 3; matrix products, arithmetic and copies ran while one was open for 2% -> 2% of each run, Pallas kernels for 0% -> 0%
where the time goes in v1:
time: 161 us
  waiting for transfers between devices  75.6 us (47%)
  blocking collectives  44.3 us (28%)
  matrix products  18 us (11%)
  between operations  14.5 us (9%)
  other arithmetic  6.86 us (4%)
    psum x1, waiting for transfers between devices, shards(): mixed = (inputs + lax.psum(head_terms, 'tp')).astype(jnp.bfloat16)  31.3 us
    psum x1, waiting for transfers between devices, shards(): up_full, total_sq2 = lax.psum((upward, squares2), 'kv')  24 us
    unnamed x4, waiting for transfers between devices  20.4 us
    unnamed x1, blocking collectives  13.5 us
    all_gather x1, blocking collectives, shards(): lax.all_gather(retained, 'kv', axis=0, tiled=True)  13.2 us
    psum x1, blocking collectives, shards(): up_full, total_sq2 = lax.psum((upward, squares2), 'kv')  11.8 us
    dot_general x4, matrix products, shards(): jnp.dot(normed, weight, preferred_element_type=jnp.float32)  6.11 us
    all_gather x1, blocking collectives, shards(): lax.all_gather(down_terms, 'tp')  5.77 us
  transfers between devices with their start and end apart: 3, of which 3 were waited for; matrix products, arithmetic and copies ran while one was open for 2% of the time, Pallas kernels for 0%

profile of v1, /device:TPU:0, one launch (start us, length us, event | category | flops | bytes accessed | tf_op | source)
XLA Modules:
  0.0 160.7 jit_solution(5920000451270685163)
XLA Ops:
  7.2 0.0 copy-start
  7.2 0.0 copy-start.2
  7.2 0.0 copy-start.3
  7.2 0.0 all-reduce.10.cloned.1.call-start
  7.2 1.6 convolution_bitcast_fusion.3
  8.8 1.5 convolution_bitcast_fusion.2
  10.3 1.5 convolution_bitcast_fusion.1
  11.8 1.5 convolution_bitcast_fusion
  13.4 0.7 pad_maximum_fusion
  14.0 0.0 all-reduce.10.cloned.1.call-update
  14.1 0.0 all-reduce.6.cloned.1.call-start
  14.1 0.9 fusion.4
  15.0 0.7 convert_element_type.40
  15.7 0.1 multiply_cosine_fusion
  15.8 1.2 dynamic-slice
  17.7 13.5 %all-reduce.1 = f32[16]{0:T(128)S(1)} all-reduce(f32[16]{0:T(128)S(1)} %fusion.4), channel_id=4, replica_groups=mesh['grp'=2,'kv'=4,'tp'=4] {'kv'}, use_global_device_ids=true, to_apply=%region_2.0.clone | all-reduce | flops 16 | bytes 128
  31.2 0.1 fusion.19
  31.3 20.3 %all-reduce.10.cloned.1.call-done = f32[16,4,512]{2,0,1:T(8,128)} async-done(((f32[16,4,512]{2,0,1:T(8,128)}), f32[16,4,512]{2,0,1:T(8,128)}) %all-reduce.10.cloned.1.call-update) | async-done | bytes 131088
  51.6 0.9 dynamic-slice_multiply_fusion
  52.5 0.1 multiply_subtract_fusion
  52.6 0.1 pad_maximum_fusion.1
  52.7 1.6 multiply_add_fusion
  54.3 0.0 copy-start.1
  54.3 1.0 fusion.22
  55.3 0.1 multiply_reduce_fusion
  55.4 0.1 fusion.17
  55.5 13.2 %all-gather.1 = bf16[4,4,512]{2,1,0:T(4,128)(2,1)S(1)} all-gather(bf16[1,4,512]{2,1,0:T(4,128)(2,1)S(1)} %reshape.109), channel_id=1, replica_groups=mesh['grp'=2,'kv'=4,'tp'=4] {'kv'}, dimensions={0}, use_global_device_ids=true | all-gather | bytes 20480 | tf_op jit(solution)/shard_map/all_gather | solution.py:67
  68.7 0.0 copy-done
  68.7 0.9 fusion.23
  69.6 0.0 all-reduce.6.cloned.1.call-update
  69.6 0.0 all-reduce.8.cloned.1.call-start
  69.6 31.3 %all-reduce.6.cloned.1.call-done = f32[16,1024]{1,0:T(8,128)} async-done(((f32[16,1024]{1,0:T(8,128)}), f32[16,1024]{1,0:T(8,128)}) %all-reduce.6.cloned.1.call-update) | async-done | bytes 65552 | tf_op jit(solution)/shard_map/psum | solution.py:71
  101.0 0.0 copy-done.2
  101.0 1.0 fusion.7
  101.9 0.0 copy-done.3
  101.9 5.3 %fusion.9 = f32[16,4096]{1,0:T(8,128)} fusion(bf16[1024,4096]{1,0:T(8,128)(2,1)} %param.22, bf16[16,1024]{1,0:T(8,128)(2,1)S(1)} %get-tuple-element.3, f32[1024]{0:T(1024)S(1)} %copy-done.3), kind=kOutput, calls=%fused_computation.22 | convolution fusion | flops 134266880 | bytes 8687616 | tf_op jit(solution)/shard_map/dot_general | solution.py:75
  107.2 0.0 copy-done.1
  107.2 0.0 all-reduce.8.cloned.1.call-update
  107.2 11.8 %psum.23 = f32[16]{0:T(128)S(1)} all-reduce(f32[16]{0:T(128)S(1)} %get-tuple-element.2), channel_id=1, replica_groups=mesh['grp'=2,'kv'=4,'tp'=4] {'kv'}, use_global_device_ids=true, to_apply=%region_7.8 | all-reduce | flops 16 | bytes 128 | tf_op jit(solution)/shard_map/psum | solution.py:76
  119.0 24.0 %all-reduce.8.cloned.1.call-done = f32[16,4096]{1,0:T(8,128)} async-done(((f32[16,4096]{1,0:T(8,128)}), f32[16,4096]{1,0:T(8,128)}) %all-reduce.8.cloned.1.call-update) | async-done | bytes 262160 | tf_op jit(solution)/shard_map/psum | solution.py:76
  143.0 4.7 %fusion = f32[16,1024]{1,0:T(8,128)S(1)} fusion(bf16[4096,1024]{1,0:T(8,128)(2,1)} %param.23, f32[16,4096]{1,0:T(8,128)} %all-reduce.8.cloned.1.call-done, f32[16]{0:T(128)S(1)} %add_rsqrt_fusion.1), kind=kOutput, calls=%fused_computation.6 | convolution fusion | flops 134479872 | bytes 8716352 | tf_op jit(solution)/shard_map/dot_general | solution.py:79
  147.7 5.8 %all-gather = f32[64,1024]{1,0:T(8,128)S(1)} all-gather(f32[16,1024]{1,0:T(8,128)S(1)} %fusion), channel_id=2, replica_groups=mesh['grp'=2,'kv'=4,'tp'=4] {'tp'}, dimensions={0}, use_global_device_ids=true | all-gather | bytes 327680 | tf_op jit(solution)/shard_map/all_gather | solution.py:80
  153.5 0.6 fusion.8
  (9 shorter events, 0.1 us)
Async XLA Ops:
  7.2 61.5 %copy-start = (bf16[512,1024]{1,0:T(8,128)(2,1)S(1)}, bf16[512,1024]{1,0:T(8,128)(2,1)}, u32[]{:S(2)}) copy-start(bf16[512,1024]{1,0:T(8,128)(2,1)} %param.20) | copy-start | bytes 3145732
  7.2 93.8 %copy-start.2 = (bf16[16,1024]{1,0:T(8,128)(2,1)S(1)}, bf16[16,1024]{1,0:T(8,128)(2,1)}, u32[]{:S(2)}) copy-start(bf16[16,1024]{1,0:T(8,128)(2,1)} %param.12) | copy-start | bytes 98308
  7.2 94.7 %copy-start.3 = (f32[1024]{0:T(1024)S(1)}, f32[1024]{0:T(1024)}, u32[]{:S(2)}) copy-start(f32[1024]{0:T(1024)} %param.21) | copy-start | bytes 12292
  7.2 44.4 %all-reduce.10.cloned.1.call-start = ((), (), s32[]{:S(2)}) async-start(), calls=%async_computation.2 | async-start | bytes 262144
  14.1 86.9 %all-reduce.6.cloned.1.call-start = ((), (), s32[]{:S(2)}) async-start(), calls=%async_computation | async-start | bytes 131072 | tf_op jit(solution)/shard_map/psum | solution.py:71
  54.3 52.9 %copy-start.1 = (f32[4,4,128,128]{3,2,1,0:T(8,128)}, f32[4,4,128,128]{3,2,1,0:T(8,128)S(1)}, u32[]{:S(2)}) copy-start(f32[4,4,128,128]{3,2,1,0:T(8,128)S(1)} %multiply_add_fusion) | copy-start | bytes 3145732
  69.6 73.4 %all-reduce.8.cloned.1.call-start = ((), (), s32[]{:S(2)}) async-start(), calls=%async_computation.1 | async-start | bytes 524288 | tf_op jit(solution)/shard_map/psum | solution.py:76
Sparse Core Ops, SparseCore 0:
  14.2 37.3 all-reduce.9
  69.7 31.1 all-reduce.5
  107.4 35.5 all-reduce.7
